TPU v7x, 32 devices: a whole 2x2x4 slice. The times are simulated.
32 devices in a mesh: sp: 8 (over z, x), tp: 4 (over y, core).
Axes of the slice: x: 2, y: 2, z: 4, core: 2. Of those that a mesh axis runs over, the one named last changes fastest.
Arguments:
- mixer_in: bfloat16 [2048, 2048], P('sp', 'tp'), may hold values from -6 to 6
- doc_ids: int32 [2048], P('sp'), may hold values from 0 to 3, never falling along the last dimension, each value on 1 to 1024 neighbouring positions
- mix_scale: float32 [2048], P('tp'), may hold values from 0.1 to 1.9
- out_proj: bfloat16 [2048, 2048], P('tp'), may hold values from -0.125 to 0.125
- residual: bfloat16 [2048, 2048], P('sp'), may hold values from -6 to 6
- mix_gain: float32 [2048], replicated, may hold values from 0.1 to 1.9
- expert_ids: int32 [2048, 2], P('sp'), may hold values from 0 to 7, all different within a row; in each aligned block of 256 rows (0 to 255, 256 to 511, ...) at most 128 rows name the same one
- expert_weight: float32 [2048, 2], P('sp'), may hold values from 0.2 to 1
- w_gate: bfloat16 [8, 2048, 5632], P('sp', None, 'tp'), may hold values from -0.125 to 0.125
- w_up: bfloat16 [8, 2048, 5632], P('sp', None, 'tp'), may hold values from -0.125 to 0.125
- w_down: bfloat16 [8, 5632, 2048], P('sp', 'tp'), may hold values from -0.078125 to 0.078125
- out_gain: float32 [2048], replicated, may hold values from 0.1 to 1.9
Outputs:
- layer_out: bfloat16 [2048, 2048], P('sp')
Inputs may be any that keep to these rules, and one draw needn't show every extreme that they name: `doc_ids`: document numbers never fall along the tokens; a document has at most 1024 positions. `expert_ids`: A row's two experts differ. In each aligned block of 256 rows (the tokens of one index of sp) no expert is named by more than 128 rows; some block has an expert named by exactly 128 rows.
All inputs are finite; a program needn't handle non-finite values.
Results may differ from a plain program's by a relative error of at most 0.015.
Values may be sent and summed in bfloat16 or wider, within the bound.
No kernel may reach another device: no remote copies, remote signals or barrier semaphores. Data moves between devices by JAX's collectives and lax.ppermute only.
A program may use at most 64 MiB of HBM per device.

v0:
```python
import jax
import jax.numpy as jnp
from jax import lax
from jax.sharding import PartitionSpec as P

alpha_res = 1.4142135623730951
norm_eps = 1e-05
pool_reach = 15


def passed_along(value, axis, steps):
    count = lax.axis_size(axis)
    initial, last = (max(0, -steps), min(count, count - steps))
    return lax.ppermute(value, axis, [(source, source + steps) for source in range(initial, last)])


def layer_norm(summed, norm_gain):
    row_mean = jnp.mean(summed, axis=-1, keepdims=True)
    centred = summed - row_mean
    row_var = jnp.mean(centred * centred, axis=-1, keepdims=True)
    return centred * lax.rsqrt(row_var + norm_eps) * norm_gain


def pair_slots(pair_ids, experts):
    flat_ids = pair_ids.reshape(-1)
    onehot = (flat_ids[:, None] == jnp.arange(experts, dtype=jnp.int32)[None, :]).astype(jnp.int32)
    before = jnp.cumsum(onehot, axis=0) - onehot
    return jnp.sum(before * onehot, axis=1).reshape(pair_ids.shape)


def shards(
    mixer_in,
    doc_ids,
    mix_scale,
    out_proj,
    residual,
    mix_gain,
    expert_ids,
    expert_weight,
    w_gate,
    w_up,
    w_down,
    out_gain,
):
    tok_rows, chan_cols = mixer_in.shape
    features = mix_gain.shape[0]
    tail_rows = (mixer_in[tok_rows - pool_reach :], doc_ids[tok_rows - pool_reach :])
    before_vals, before_doc = passed_along((tail_rows[0], tail_rows[1]), "sp", 1)
    extended = jnp.concatenate([before_vals, mixer_in], axis=0).astype(jnp.float32)
    extended_doc = jnp.concatenate([before_doc, doc_ids], axis=0)
    positions = lax.axis_index("sp") * tok_rows + jnp.arange(tok_rows, dtype=jnp.int32)
    channel = lax.axis_index("tp") * chan_cols + jnp.arange(chan_cols, dtype=jnp.int32)
    window = jnp.left_shift(jnp.int32(2), channel // (features // 4))
    window_sum = jnp.zeros((tok_rows, chan_cols), jnp.float32)
    window_count = jnp.zeros((tok_rows, chan_cols), jnp.float32)
    for lag_step in range(pool_reach + 1):
        shifted = extended[pool_reach - lag_step : pool_reach - lag_step + tok_rows]
        same_doc = (
            extended_doc[pool_reach - lag_step : pool_reach - lag_step + tok_rows] == doc_ids
        ) & (positions >= lag_step)
        in_window = (same_doc[:, None] & (lag_step < window)[None, :]).astype(jnp.float32)
        window_sum = window_sum + in_window * shifted
        window_count = window_count + in_window
    mixed_rows = ((window_sum / window_count - extended[pool_reach:]) * mix_scale).astype(
        jnp.bfloat16
    )
    share_rows = tok_rows // lax.axis_size("tp")
    projected = lax.psum_scatter(
        jnp.dot(mixed_rows, out_proj, preferred_element_type=jnp.float32).astype(jnp.bfloat16),
        "tp",
        scatter_dimension=0,
        tiled=True,
    ).astype(jnp.float32)
    own_residual = lax.dynamic_slice_in_dim(
        residual, lax.axis_index("tp") * share_rows, share_rows, 0
    )
    normed_share = layer_norm(
        alpha_res * own_residual.astype(jnp.float32) + projected, mix_gain
    ).astype(jnp.bfloat16)
    normed = lax.all_gather(normed_share, "tp", axis=0, tiled=True)
    experts = lax.axis_size("sp")
    capacity = 4 * tok_rows // experts
    ranks = pair_slots(expert_ids, experts)
    target = expert_ids * capacity + ranks
    slot_ids = jnp.arange(experts * capacity, dtype=jnp.int32)[:, None]
    select = ((target[None, :, 0] == slot_ids) | (target[None, :, 1] == slot_ids)).astype(
        jnp.bfloat16
    )
    source_rows = lax.dynamic_slice_in_dim(normed, lax.axis_index("tp") * chan_cols, chan_cols, 1)
    outgoing = jnp.dot(select, source_rows, preferred_element_type=jnp.float32).astype(jnp.bfloat16)
    outgoing = outgoing.reshape(experts, capacity, source_rows.shape[1])
    incoming = lax.all_to_all(outgoing, "sp", split_axis=0, concat_axis=0, tiled=True)
    incoming = lax.all_gather(incoming, "tp", axis=2, tiled=True)
    senders, slot_count, width_all = incoming.shape
    flat_in = incoming.reshape(senders * slot_count, width_all)
    gate_pre = jnp.dot(flat_in, w_gate[0], preferred_element_type=jnp.float32)
    upper = jnp.dot(flat_in, w_up[0], preferred_element_type=jnp.float32)
    hidden = (jax.nn.silu(gate_pre) * upper).astype(jnp.bfloat16)
    partial_value = jnp.dot(hidden, w_down[0], preferred_element_type=jnp.float32).astype(
        jnp.bfloat16
    )
    returned = lax.all_to_all(
        partial_value.reshape(senders, slot_count, width_all),
        "sp",
        split_axis=0,
        concat_axis=0,
        tiled=True,
    )
    picked = returned.reshape(experts * capacity, features)[target]
    weighted = jnp.sum(picked.astype(jnp.float32) * expert_weight[:, :, None], axis=1)
    routed = lax.psum(weighted.astype(jnp.bfloat16), "tp").astype(jnp.float32)
    return layer_norm(alpha_res * normed.astype(jnp.float32) + routed, out_gain).astype(
        jnp.bfloat16
    )


def solution(mesh):
    placed = (
        P("sp", "tp"),
        P("sp"),
        P("tp"),
        P("tp", None),
        P("sp", None),
        P(),
        P("sp", None),
        P("sp", None),
        P("sp", None, "tp"),
        P("sp", None, "tp"),
        P("sp", "tp", None),
        P(),
    )
    return jax.shard_map(
        shards, mesh=mesh, in_specs=placed, out_specs=P("sp", None), check_vma=False
    )
```

profile of v0, /device:TPU:0, one launch (start us, length us, event | category | flops | bytes accessed | tf_op | source)
XLA Modules:
  0.0 340.1 jit_solution(10196914106169270172)
XLA Ops:
  7.4 4.9 %collective-permute-start.1 = (s32[15]{0:T(128)S(1)}, s32[15]{0:T(128)S(1)}, u32[]{:S(2)}, u32[]{:S(2)}) collective-permute-start(s32[15]{0:T(128)S(1)} %slice.114), channel_id=1, source_target_pairs={{0,4},{4,8},{8,12},{12,16},{16,20},{20,24},{24,28},{1,5},{5,9},{9,... | collective-permute-start | bytes 188 | tf_op jit(solution)/shard_map/ppermute | solution.py:14
  13.0 3.4 %collective-permute-start = (bf16[15,512]{1,0:T(8,128)(2,1)S(1)}, bf16[15,512]{1,0:T(8,128)(2,1)S(1)}, u32[]{:S(2)}, u32[]{:S(2)}) collective-permute-start(bf16[15,512]{1,0:T(8,128)(2,1)S(1)} %slice.112), channel_id=1, source_target_pairs={{0,4},{4,8},{8,12},{12,16},{16,20},{20,24},{24,28},{1,5},{5,9},{9,... | collective-permute-start | bytes 46088 | tf_op jit(solution)/shard_map/ppermute | solution.py:14
  18.2 1.0 maximum_convert_fusion
  19.3 5.9 %convolution_convert_fusion = bf16[256,2048]{1,0:T(8,128)(2,1)} fusion(bf16[512,2048]{1,0:T(8,128)(2,1)S(1)} %copy-done, f32[271,512]{1,0:T(8,128)S(1)} %maximum_convert_fusion, f32[512]{0:T(512)} %param.14, pred[512]{0:T(512)(128)(4,1)S(1)} %get-tuple-element.24, pred[512]{0:T(512)(128)(4,1)S(1)} %get-tuple-element.25, ...), kind=kOutput, calls=%fused_computation.11 | convolution fusion | flops 548143104 | bytes 11552768 | tf_op jit(solution)/shard_map/dot_general | solution.py:69
  25.3 26.5 %reduce-scatter.2.cloned.1.call-done = bf16[64,2048]{1,0:T(8,128)(2,1)} async-done(((bf16[256,2048]{1,0:T(8,128)(2,1)}), bf16[64,2048]{1,0:T(8,128)(2,1)}) %reduce-scatter.2.cloned.1.call-update) | async-done | bytes 262160 | tf_op jit(solution)/shard_map/reduce_scatter | solution.py:68
  51.8 1.1 fusion.53
  53.0 1.2 multiply_reduce_fusion.2
  54.2 1.8 multiply_convert_fusion.2
  56.5 1.1 reduce-window.6
  58.2 14.7 %all-gather.3.cloned.1.call-done = bf16[256,2048]{1,0:T(8,128)(2,1)} async-done(((bf16[64,2048]{1,0:T(8,128)(2,1)}), bf16[256,2048]{1,0:T(8,128)(2,1)}) %all-gather.3.cloned.1.call-update) | async-done | bytes 1048592 | tf_op jit(solution)/shard_map/all_gather | solution.py:80
  72.9 1.4 convolution_convert_fusion.1
  74.3 31.5 %all_to_all.10 = bf16[8,128,512]{2,1,0:T(8,128)(2,1)} all-to-all(bf16[8,128,512]{2,1,0:T(8,128)(2,1)S(1)} %bitcast.35), channel_id=1, replica_groups=mesh['sp'=8,'tp'=4] {'sp'}, dimensions={0} | all-to-all | bytes 2097152 | tf_op jit(solution)/shard_map/all_to_all | solution.py:92
  105.9 32.7 %all-gather.5.cloned.1.call-done = bf16[8,128,2048]{2,1,0:T(8,128)(2,1)} async-done(((bf16[8,128,512]{2,1,0:T(8,128)(2,1)}), bf16[8,128,2048]{2,1,0:T(8,128)(2,1)}) %all-gather.5.cloned.1.call-update) | async-done | bytes 4194320 | tf_op jit(solution)/shard_map/all_gather | solution.py:93
  138.6 11.7 %fusion.4 = f32[1024,1408]{1,0:T(8,128)} fusion(bf16[1024,2048]{1,0:T(8,128)(2,1)} %bitcast.38, bf16[1,2048,1408]{2,1,0:T(8,128)(2,1)} %param.20), kind=kOutput, calls=%fused_computation.5 | convolution fusion | flops 5905580032 | bytes 15728640 | tf_op jit(solution)/shard_map/dot_general | solution.py:96
  150.3 20.6 %fusion.10 = bf16[1024,2048]{1,0:T(8,128)(2,1)} fusion(bf16[1,1408,2048]{2,1,0:T(8,128)(2,1)} %param.22, f32[1024,1408]{1,0:T(8,128)} %fusion.4, bf16[1024,2048]{1,0:T(8,128)(2,1)} %bitcast.39, bf16[1,2048,1408]{2,1,0:T(8,128)(2,1)} %param.21), kind=kOutput, calls=%fused_computation.9 | convolution fusion | flops 11821907968 | bytes 25690112 | tf_op jit(solution)/shard_map/dot_general | solution.py:99
  171.0 5.6 %all-to-all-start.1 = ((bf16[8,128,2048]{2,1,0:T(8,128)(2,1)}), bf16[8,128,2048]{2,1,0:T(8,128)(2,1)}, u32[]{:S(2)}, u32[]{:S(2)}) async-start(bf16[8,128,2048]{2,1,0:T(8,128)(2,1)} %bitcast.34), calls=%async_computation.2 | async-start | bytes 8388608 | tf_op jit(solution)/shard_map/all_to_all | solution.py:102
  177.1 93.2 %all-to-all-done.1 = bf16[8,128,2048]{2,1,0:T(8,128)(2,1)} async-done(((bf16[8,128,2048]{2,1,0:T(8,128)(2,1)}), bf16[8,128,2048]{2,1,0:T(8,128)(2,1)}, u32[]{:S(2)}, u32[]{:S(2)}) %all-to-all-start.1) | async-done | bytes 4194336 | tf_op jit(solution)/shard_map/all_to_all | solution.py:102
  270.3 8.2 %gather_fusion = bf16[512,2048]{1,0:T(8,128)(2,1)} fusion(bf16[1024,2048]{1,0:T(8,128)(2,1)} %bitcast.10, s32[1024]{0:T(1024)S(1)} %pad_clamp_fusion), kind=kCustom, calls=%fused_computation | custom fusion | bytes 4196352 | tf_op jit(solution)/shard_map/gather | solution.py:109
  278.5 5.4 %reshape.164 = f32[256,2,2048]{2,1,0:T(2,128)} reshape(bf16[512,2048]{1,0:T(8,128)(2,1)} %gather_fusion) | data formatting | bytes 6291456 | tf_op jit(solution)/shard_map/convert_element_type | solution.py:110
  283.9 9.9 %multiply_reduce_fusion = bf16[256,2048]{1,0:T(8,128)(2,1)} fusion(f32[256,2,2048]{2,1,0:T(2,128)} %reshape.164, f32[256,2]{1,0:T(8,128)S(1)} %copy.28), kind=kLoop, calls=%fused_computation.8 | loop fusion | flops 1572864 | bytes 5244928 | tf_op jit(solution)/shard_map/reduce_sum | solution.py:110
  293.9 34.6 %all-reduce.2.cloned.1.call-done = bf16[256,2048]{1,0:T(8,128)(2,1)} async-done(((bf16[256,2048]{1,0:T(8,128)(2,1)}), bf16[256,2048]{1,0:T(8,128)(2,1)}) %all-reduce.2.cloned.1.call-update) | async-done | bytes 1048592 | tf_op jit(solution)/shard_map/psum | solution.py:111
  328.5 1.7 fusion.16
  330.2 1.8 multiply_reduce_fusion.1
  332.0 1.5 multiply_convert_fusion.1
  (58 shorter events, 4.9 us)
Async XLA Ops:
  6.5 12.7 %copy-start = (bf16[512,2048]{1,0:T(8,128)(2,1)S(1)}, bf16[512,2048]{1,0:T(8,128)(2,1)}, u32[]{:S(2)}) copy-start(bf16[512,2048]{1,0:T(8,128)(2,1)} %param.15) | copy-start | bytes 6291460
  6.5 45.3 %reduce-scatter.2.cloned.1.call-start = ((), (), s32[]{:S(2)}) async-start(), calls=%async_computation.3 | async-start | bytes 1310720 | tf_op jit(solution)/shard_map/reduce_scatter | solution.py:68
  7.4 9.2 %collective-permute-start.1 = (s32[15]{0:T(128)S(1)}, s32[15]{0:T(128)S(1)}, u32[]{:S(2)}, u32[]{:S(2)}) collective-permute-start(s32[15]{0:T(128)S(1)} %slice.114), channel_id=1, source_target_pairs={{0,4},{4,8},{8,12},{12,16},{16,20},{20,24},{24,28},{1,5},{5,9},{9,... | collective-permute-start | bytes 188 | tf_op jit(solution)/shard_map/ppermute | solution.py:14
  13.0 5.2 %collective-permute-start = (bf16[15,512]{1,0:T(8,128)(2,1)S(1)}, bf16[15,512]{1,0:T(8,128)(2,1)S(1)}, u32[]{:S(2)}, u32[]{:S(2)}) collective-permute-start(bf16[15,512]{1,0:T(8,128)(2,1)S(1)} %slice.112), channel_id=1, source_target_pairs={{0,4},{4,8},{8,12},{12,16},{16,20},{20,24},{24,28},{1,5},{5,9},{9,... | collective-permute-start | bytes 46088 | tf_op jit(solution)/shard_map/ppermute | solution.py:14
  19.2 32.6 %copy-start.3 = (bf16[256,2048]{1,0:T(8,128)(2,1)S(1)}, bf16[256,2048]{1,0:T(8,128)(2,1)}, u32[]{:S(2)}) copy-start(bf16[256,2048]{1,0:T(8,128)(2,1)} %param.16) | copy-start | bytes 3145732
  19.3 34.9 %copy-start.4 = (f32[2048]{0:T(1024)S(1)}, f32[2048]{0:T(1024)}, u32[]{:S(2)}) copy-start(f32[2048]{0:T(1024)} %param.17) | copy-start | bytes 24580
  19.3 36.8 %copy-start.6 = (s32[256,2]{0,1:T(2,128)S(1)}, s32[256,2]{0,1:T(2,128)}, u32[]{:S(2)}) copy-start(s32[256,2]{0,1:T(2,128)} %param.18) | copy-start | bytes 6148
  25.2 47.7 %all-gather.3.cloned.1.call-start = ((), (), s32[]{:S(2)}) async-start(), calls=%async_computation.4 | async-start | bytes 1310720 | tf_op jit(solution)/shard_map/all_gather | solution.py:80
  56.0 82.6 %all-gather.5.cloned.1.call-start = ((), (), s32[]{:S(2)}) async-start(), calls=%async_computation.5 | async-start | bytes 5242880 | tf_op jit(solution)/shard_map/all_gather | solution.py:93
  171.0 6.0 %copy-start.7 = (f32[256,2]{0,1:T(2,128)S(1)}, f32[256,2]{0,1:T(2,128)}, u32[]{:S(2)}) copy-start(f32[256,2]{0,1:T(2,128)} %param.19) | copy-start | bytes 6148
  171.0 99.3 %all-to-all-start.1 = ((bf16[8,128,2048]{2,1,0:T(8,128)(2,1)}), bf16[8,128,2048]{2,1,0:T(8,128)(2,1)}, u32[]{:S(2)}, u32[]{:S(2)}) async-start(bf16[8,128,2048]{2,1,0:T(8,128)(2,1)} %bitcast.34), calls=%async_computation.2 | async-start | bytes 8388608 | tf_op jit(solution)/shard_map/all_to_all | solution.py:102
  176.6 151.8 %all-reduce.2.cloned.1.call-start = ((), (), s32[]{:S(2)}) async-start(), calls=%async_computation.6 | async-start | bytes 2097152 | tf_op jit(solution)/shard_map/psum | solution.py:111
  283.9 44.5 %copy-start.1 = (bf16[256,2048]{1,0:T(8,128)(2,1)S(1)}, bf16[256,2048]{1,0:T(8,128)(2,1)}, u32[]{:S(2)}) copy-start(bf16[256,2048]{1,0:T(8,128)(2,1)} %all-gather.3.cloned.1.call-done) | copy-start | bytes 3145732
  283.9 48.1 %copy-start.5 = (f32[2048]{0:T(1024)S(1)}, f32[2048]{0:T(1024)}, u32[]{:S(2)}) copy-start(f32[2048]{0:T(1024)} %param.23) | copy-start | bytes 24580
  328.4 3.5 %copy-start.2 = (bf16[256,2048]{1,0:T(8,128)(2,1)S(1)}, bf16[256,2048]{1,0:T(8,128)(2,1)}, u32[]{:S(2)}) copy-start(bf16[256,2048]{1,0:T(8,128)(2,1)} %all-reduce.2.cloned.1.call-done) | copy-start | bytes 3145732
Sparse Core Ops, SparseCore 0:
  25.3 26.4 reduce-scatter.1
  56.1 16.7 all-gather.2
  106.0 32.5 all-gather.4
  294.0 34.4 all-reduce.1
where the time goes:
time: 341 us; the launch traced here: 340 us
  waiting for transfers between devices  202 us (59%)
  matrix products  39.7 us (12%)
  blocking collectives  31.5 us (9%)
  other arithmetic  23.1 us (7%)
  local copies, waits for them, and re-layouts  16.5 us (5%)
  starting transfers between devices  14.1 us (4%)
  between operations  13.4 us (4%)
    all_to_all x1, waiting for transfers between devices, shards(): lax.all_to_all(partial_value.reshape(senders, slot_count, width_all), 'sp...  93.2 us
    psum x1, waiting for transfers between devices, shards(): routed = lax.psum(weighted.astype(jnp.bfloat16), 'tp').astype(jnp.float32)  34.6 us
    all_gather x1, waiting for transfers between devices, shards(): incoming = lax.all_gather(incoming, 'tp', axis=2, tiled=True)  32.7 us
    all_to_all x1, blocking collectives, shards(): lax.all_to_all(outgoing, 'sp', split_axis=0, concat_axis=0, tiled=True)  31.5 us
    reduce_scatter x1, waiting for transfers between devices, shards(): lax.psum_scatter(jnp.dot(mixed_rows, out_proj, preferred_element_type=jnp...  26.5 us
    dot_general x1, matrix products, shards(): jnp.dot(hidden, w_down[0], preferred_element_type=jnp.float32)  20.6 us
    all_gather x1, waiting for transfers between devices, shards(): normed = lax.all_gather(normed_share, 'tp', axis=0, tiled=True)  14.7 us
    dot_general x1, matrix products, shards(): gate_pre = jnp.dot(flat_in, w_gate[0], preferred_element_type=jnp.float32)  11.7 us
  transfers between devices with their start and end apart: 7, of which 5 were waited for; matrix products, arithmetic and copies ran while one was open for 1% of the time, Pallas kernels for 0%

commit v1 on v0

--- a/solution.py
+++ b/solution.py
@@ -108,7 +108,9 @@
     )
     picked = returned.reshape(experts * capacity, features)[target]
     weighted = jnp.sum(picked.astype(jnp.float32) * expert_weight[:, :, None], axis=1)
-    routed = lax.psum(weighted.astype(jnp.bfloat16), "tp").astype(jnp.float32)
+    routed = jnp.sum(lax.all_gather(weighted.astype(jnp.bfloat16), "tp"), axis=0).astype(
+        jnp.float32
+    )
     return layer_norm(alpha_res * normed.astype(jnp.float32) + routed, out_gain).astype(
         jnp.bfloat16
     )

time: 341 us -> 342 us (level)
    psum x1 -> x0, waiting for transfers between devices: 34.6 us -> none  [shards(): routed = lax.psum(weighted.astype(jnp.bfloat16), 'tp').astype(jnp.float32)]
    all_gather x0 -> x1, waiting for transfers between devices: none -> 32.7 us  [shards(): lax.all_gather(weighted.astype(jnp.bfloat16), 'tp')]
where the time goes in v1:
time: 342 us; the launch traced here: 341 us
  waiting for transfers between devices  200 us (58%)
  matrix products  39.7 us (12%)
  blocking collectives  31.5 us (9%)
  other arithmetic  26.1 us (8%)
  local copies, waits for them, and re-layouts  16.4 us (5%)
  starting transfers between devices  14.2 us (4%)
  between operations  13.4 us (4%)
    all_to_all x1, waiting for transfers between devices, shards(): lax.all_to_all(partial_value.reshape(senders, slot_count, width_all), 'sp...  93 us
    all_gather x1, waiting for transfers between devices, shards(): lax.all_gather(weighted.astype(jnp.bfloat16), 'tp')  32.7 us
    all_gather x1, waiting for transfers between devices, shards(): incoming = lax.all_gather(incoming, 'tp', axis=2, tiled=True)  32.7 us
    all_to_all x1, blocking collectives, shards(): lax.all_to_all(outgoing, 'sp', split_axis=0, concat_axis=0, tiled=True)  31.5 us
    reduce_scatter x1, waiting for transfers between devices, shards(): lax.psum_scatter(jnp.dot(mixed_rows, out_proj, preferred_element_type=jnp...  26.5 us
    dot_general x1, matrix products, shards(): jnp.dot(hidden, w_down[0], preferred_element_type=jnp.float32)  20.6 us
    all_gather x1, waiting for transfers between devices, shards(): normed = lax.all_gather(normed_share, 'tp', axis=0, tiled=True)  14.7 us
    dot_general x1, matrix products, shards(): gate_pre = jnp.dot(flat_in, w_gate[0], preferred_element_type=jnp.float32)  11.7 us
  transfers between devices with their start and end apart: 7, of which 5 were waited for; matrix products, arithmetic and copies ran while one was open for 1% of the time, Pallas kernels for 0%

profile of v1, /device:TPU:0, one launch (start us, length us, event | category | flops | bytes accessed | tf_op | source)
XLA Modules:
  0.0 341.1 jit_solution(4069595140298673198)
XLA Ops:
  7.4 4.9 %collective-permute-start.1 = (s32[15]{0:T(128)S(1)}, s32[15]{0:T(128)S(1)}, u32[]{:S(2)}, u32[]{:S(2)}) collective-permute-start(s32[15]{0:T(128)S(1)} %slice.114), channel_id=1, source_target_pairs={{0,4},{4,8},{8,12},{12,16},{16,20},{20,24},{24,28},{1,5},{5,9},{9,... | collective-permute-start | bytes 188 | tf_op jit(solution)/shard_map/ppermute | solution.py:14
  13.0 3.4 %collective-permute-start = (bf16[15,512]{1,0:T(8,128)(2,1)S(1)}, bf16[15,512]{1,0:T(8,128)(2,1)S(1)}, u32[]{:S(2)}, u32[]{:S(2)}) collective-permute-start(bf16[15,512]{1,0:T(8,128)(2,1)S(1)} %slice.112), channel_id=1, source_target_pairs={{0,4},{4,8},{8,12},{12,16},{16,20},{20,24},{24,28},{1,5},{5,9},{9,... | collective-permute-start | bytes 46088 | tf_op jit(solution)/shard_map/ppermute | solution.py:14
  19.3 5.9 %convolution_convert_fusion = bf16[256,2048]{1,0:T(8,128)(2,1)} fusion(bf16[512,2048]{1,0:T(8,128)(2,1)S(1)} %copy-done, f32[271,512]{1,0:T(8,128)S(1)} %maximum_convert_fusion, f32[512]{0:T(512)} %param.14, pred[512]{0:T(512)(128)(4,1)S(1)} %get-tuple-element.24, pred[512]{0:T(512)(128)(4,1)S(1)} %get-tuple-element.25, ...), kind=kOutput, calls=%fused_computation.11 | convolution fusion | flops 548143104 | bytes 11552768 | tf_op jit(solution)/shard_map/dot_general | solution.py:69
  25.3 26.5 %reduce-scatter.2.cloned.1.call-done = bf16[64,2048]{1,0:T(8,128)(2,1)} async-done(((bf16[256,2048]{1,0:T(8,128)(2,1)}), bf16[64,2048]{1,0:T(8,128)(2,1)}) %reduce-scatter.2.cloned.1.call-update) | async-done | bytes 262160 | tf_op jit(solution)/shard_map/reduce_scatter | solution.py:68
  51.8 1.1 fusion.53
  53.0 1.2 multiply_reduce_fusion.2
  54.2 1.8 multiply_convert_fusion.2
  56.5 1.1 reduce-window.6
  58.2 14.7 %all-gather.5.cloned.1.call-done = bf16[256,2048]{1,0:T(8,128)(2,1)} async-done(((bf16[64,2048]{1,0:T(8,128)(2,1)}), bf16[256,2048]{1,0:T(8,128)(2,1)}) %all-gather.5.cloned.1.call-update) | async-done | bytes 1048592 | tf_op jit(solution)/shard_map/all_gather | solution.py:80
  72.9 1.4 convolution_convert_fusion.1
  74.3 31.5 %all_to_all.10 = bf16[8,128,512]{2,1,0:T(8,128)(2,1)} all-to-all(bf16[8,128,512]{2,1,0:T(8,128)(2,1)S(1)} %bitcast.37), channel_id=1, replica_groups=mesh['sp'=8,'tp'=4] {'sp'}, dimensions={0} | all-to-all | bytes 2097152 | tf_op jit(solution)/shard_map/all_to_all | solution.py:92
  105.9 32.7 %all-gather.7.cloned.1.call-done = bf16[8,128,2048]{2,1,0:T(8,128)(2,1)} async-done(((bf16[8,128,512]{2,1,0:T(8,128)(2,1)}), bf16[8,128,2048]{2,1,0:T(8,128)(2,1)}) %all-gather.7.cloned.1.call-update) | async-done | bytes 4194320 | tf_op jit(solution)/shard_map/all_gather | solution.py:93
  138.6 11.7 %fusion.4 = f32[1024,1408]{1,0:T(8,128)} fusion(bf16[1024,2048]{1,0:T(8,128)(2,1)} %bitcast.40, bf16[1,2048,1408]{2,1,0:T(8,128)(2,1)} %param.20), kind=kOutput, calls=%fused_computation.5 | convolution fusion | flops 5905580032 | bytes 15728640 | tf_op jit(solution)/shard_map/dot_general | solution.py:96
  150.3 20.6 %fusion.10 = bf16[1024,2048]{1,0:T(8,128)(2,1)} fusion(bf16[1,1408,2048]{2,1,0:T(8,128)(2,1)} %param.22, f32[1024,1408]{1,0:T(8,128)} %fusion.4, bf16[1024,2048]{1,0:T(8,128)(2,1)} %bitcast.41, bf16[1,2048,1408]{2,1,0:T(8,128)(2,1)} %param.21), kind=kOutput, calls=%fused_computation.9 | convolution fusion | flops 11821907968 | bytes 25690112 | tf_op jit(solution)/shard_map/dot_general | solution.py:99
  171.0 5.6 %all-to-all-start.1 = ((bf16[8,128,2048]{2,1,0:T(8,128)(2,1)}), bf16[8,128,2048]{2,1,0:T(8,128)(2,1)}, u32[]{:S(2)}, u32[]{:S(2)}) async-start(bf16[8,128,2048]{2,1,0:T(8,128)(2,1)} %bitcast.35), calls=%async_computation.2 | async-start | bytes 8388608 | tf_op jit(solution)/shard_map/all_to_all | solution.py:102
  177.3 93.0 %all-to-all-done.1 = bf16[8,128,2048]{2,1,0:T(8,128)(2,1)} async-done(((bf16[8,128,2048]{2,1,0:T(8,128)(2,1)}), bf16[8,128,2048]{2,1,0:T(8,128)(2,1)}, u32[]{:S(2)}, u32[]{:S(2)}) %all-to-all-start.1) | async-done | bytes 4194336 | tf_op jit(solution)/shard_map/all_to_all | solution.py:102
  270.3 8.0 %gather_fusion = bf16[512,2048]{1,0:T(8,128)(2,1)} fusion(bf16[1024,2048]{1,0:T(8,128)(2,1)} %bitcast.10, s32[1024]{0:T(1024)S(1)} %pad_clamp_fusion), kind=kCustom, calls=%fused_computation | custom fusion | bytes 4196352 | tf_op jit(solution)/shard_map/gather | solution.py:109
  278.3 5.4 %reshape.173 = f32[256,2,2048]{2,1,0:T(2,128)} reshape(bf16[512,2048]{1,0:T(8,128)(2,1)} %gather_fusion) | data formatting | bytes 6291456 | tf_op jit(solution)/shard_map/convert_element_type | solution.py:110
  283.7 9.9 %multiply_reduce_fusion = bf16[256,2048]{1,0:T(8,128)(2,1)} fusion(f32[256,2,2048]{2,1,0:T(2,128)} %reshape.173, f32[256,2]{1,0:T(8,128)S(1)} %copy.33), kind=kLoop, calls=%fused_computation.8 | loop fusion | flops 1572864 | bytes 5244928 | tf_op jit(solution)/shard_map/reduce_sum | solution.py:110
  293.6 32.7 %all-gather.9.cloned.1.call-done = bf16[1024,2048]{1,0:T(8,128)(2,1)} async-done(((bf16[256,2048]{1,0:T(8,128)(2,1)}), bf16[1024,2048]{1,0:T(8,128)(2,1)}) %all-gather.9.cloned.1.call-update) | async-done | bytes 4194320 | tf_op jit(solution)/shard_map/all_gather | solution.py:111
  326.4 3.1 reduce_sum.70
  329.5 1.7 fusion.16
  331.2 1.8 multiply_reduce_fusion.1
  333.0 1.5 multiply_convert_fusion.1
  (57 shorter events, 6.1 us)
Async XLA Ops:
  6.5 12.7 %copy-start = (bf16[512,2048]{1,0:T(8,128)(2,1)S(1)}, bf16[512,2048]{1,0:T(8,128)(2,1)}, u32[]{:S(2)}) copy-start(bf16[512,2048]{1,0:T(8,128)(2,1)} %param.15) | copy-start | bytes 6291460
  6.5 45.3 %reduce-scatter.2.cloned.1.call-start = ((), (), s32[]{:S(2)}) async-start(), calls=%async_computation.3 | async-start | bytes 1310720 | tf_op jit(solution)/shard_map/reduce_scatter | solution.py:68
  7.4 9.2 %collective-permute-start.1 = (s32[15]{0:T(128)S(1)}, s32[15]{0:T(128)S(1)}, u32[]{:S(2)}, u32[]{:S(2)}) collective-permute-start(s32[15]{0:T(128)S(1)} %slice.114), channel_id=1, source_target_pairs={{0,4},{4,8},{8,12},{12,16},{16,20},{20,24},{24,28},{1,5},{5,9},{9,... | collective-permute-start | bytes 188 | tf_op jit(solution)/shard_map/ppermute | solution.py:14
  13.0 5.2 %collective-permute-start = (bf16[15,512]{1,0:T(8,128)(2,1)S(1)}, bf16[15,512]{1,0:T(8,128)(2,1)S(1)}, u32[]{:S(2)}, u32[]{:S(2)}) collective-permute-start(bf16[15,512]{1,0:T(8,128)(2,1)S(1)} %slice.112), channel_id=1, source_target_pairs={{0,4},{4,8},{8,12},{12,16},{16,20},{20,24},{24,28},{1,5},{5,9},{9,... | collective-permute-start | bytes 46088 | tf_op jit(solution)/shard_map/ppermute | solution.py:14
  19.2 32.6 %copy-start.2 = (bf16[256,2048]{1,0:T(8,128)(2,1)S(1)}, bf16[256,2048]{1,0:T(8,128)(2,1)}, u32[]{:S(2)}) copy-start(bf16[256,2048]{1,0:T(8,128)(2,1)} %param.16) | copy-start | bytes 3145732
  19.3 34.9 %copy-start.3 = (f32[2048]{0:T(1024)S(1)}, f32[2048]{0:T(1024)}, u32[]{:S(2)}) copy-start(f32[2048]{0:T(1024)} %param.17) | copy-start | bytes 24580
  19.3 36.8 %copy-start.5 = (s32[256,2]{0,1:T(2,128)S(1)}, s32[256,2]{0,1:T(2,128)}, u32[]{:S(2)}) copy-start(s32[256,2]{0,1:T(2,128)} %param.18) | copy-start | bytes 6148
  25.2 47.7 %all-gather.5.cloned.1.call-start = ((), (), s32[]{:S(2)}) async-start(), calls=%async_computation.4 | async-start | bytes 1310720 | tf_op jit(solution)/shard_map/all_gather | solution.py:80
  56.0 82.6 %all-gather.7.cloned.1.call-start = ((), (), s32[]{:S(2)}) async-start(), calls=%async_computation.5 | async-start | bytes 5242880 | tf_op jit(solution)/shard_map/all_gather | solution.py:93
  171.0 6.2 %copy-start.6 = (f32[256,2]{0,1:T(2,128)S(1)}, f32[256,2]{0,1:T(2,128)}, u32[]{:S(2)}) copy-start(f32[256,2]{0,1:T(2,128)} %param.19) | copy-start | bytes 6148
  171.0 99.3 %all-to-all-start.1 = ((bf16[8,128,2048]{2,1,0:T(8,128)(2,1)}), bf16[8,128,2048]{2,1,0:T(8,128)(2,1)}, u32[]{:S(2)}, u32[]{:S(2)}) async-start(bf16[8,128,2048]{2,1,0:T(8,128)(2,1)} %bitcast.35), calls=%async_computation.2 | async-start | bytes 8388608 | tf_op jit(solution)/shard_map/all_to_all | solution.py:102
  176.6 149.7 %all-gather.9.cloned.1.call-start = ((), (), s32[]{:S(2)}) async-start(), calls=%async_computation.6 | async-start | bytes 5242880 | tf_op jit(solution)/shard_map/all_gather | solution.py:111
  326.4 6.6 %copy-start.4 = (f32[2048]{0:T(1024)S(1)}, f32[2048]{0:T(1024)}, u32[]{:S(2)}) copy-start(f32[2048]{0:T(1024)} %param.23) | copy-start | bytes 24580
  329.5 3.6 %copy-start.1 = (bf16[256,2048]{1,0:T(8,128)(2,1)S(1)}, bf16[256,2048]{1,0:T(8,128)(2,1)}, u32[]{:S(2)}) copy-start(bf16[256,2048]{1,0:T(8,128)(2,1)} %all-gather.5.cloned.1.call-done) | copy-start | bytes 3145732
Sparse Core Ops, SparseCore 0:
  25.3 26.4 reduce-scatter.1
  56.1 16.7 all-gather.4
  106.0 32.5 all-gather.6
  293.7 32.5 all-gather.8
